TPU v7x, 1024 devices: a whole 4x4x32 slice. The times are simulated.
1024 devices in a mesh: rep: 4 (over z_hi), fs: 32 (over z_lo, y), tp: 8 (over x, core).
Axes of the slice: x: 4, y: 4, z: 32 (z_hi: 4, z_lo: 8; z = z_hi * 8 + z_lo), core: 2. Of those that a mesh axis runs over, the one named last changes fastest.
Arguments:
- skip_stream_entry: bfloat16 [32768, 2048], P(('rep', 'fs')), may hold values from -6 to 6
- sequence_blender_factor: float32 [2048], replicated, may hold values from 0.1 to 1.9
- product_projector: float32 [2048, 1024], P('fs', 'tp'), may hold values from -0.125 to 0.125
- product_side_factors: float32 [1024], P('tp'), may hold values from 0.3 to 3
- placewise_projector: float32 [2048, 1024], P('fs', 'tp'), may hold values from -0.125 to 0.125
- placewise_entry_factors: float32 [1024], P('tp'), may hold values from 0.7 to 11.2, as said below
- placewise_rescale_factor: float32 [1024], P('tp'), may hold values from 0.1 to 1.9
- place_cluster_operator: bfloat16 [8, 128, 128], replicated, may hold values from -0.5 to 0.5
- placewise_offset_vector: float32 [8, 128], replicated, may hold values from 0.1 to 1.9
- blender_result_projector: float32 [1024, 2048], P('tp', 'fs'), may hold values from -0.1875 to 0.1875
- blender_result_factors: float32 [2048], P('fs'), may hold values from 0.3 to 3
- feedforward_norm_factor: float32 [2048], replicated, may hold values from 0.1 to 1.9
- switch_projector: float32 [2048, 2816], P('fs', 'tp'), may hold values from -0.125 to 0.125
- switch_factors: float32 [2816], P('tp'), may hold values from 0.3 to 3
- expand_projector: float32 [2048, 2816], P('fs', 'tp'), may hold values from -0.125 to 0.125
- expand_factors: float32 [2816], P('tp'), may hold values from 0.3 to 3
- contract_projector: float32 [2816, 2048], P('tp', 'fs'), may hold values from -0.109375 to 0.109375
- contract_factors: float32 [2048], P('fs'), may hold values from 0.3 to 3
Outputs:
- result: bfloat16 [32768, 2048], P(('rep', 'fs'), 'tp')
Inputs may be any that keep to these rules, and one draw needn't show every extreme that they name: `placewise_entry_factors`: positive column scales.
All inputs are finite; a program needn't handle non-finite values.
Results may differ from a plain program's by a relative error of at most 0.023.
Values may be sent and summed in bfloat16 or wider, within the bound.
A program may use at most 32 MiB of HBM per device.

v0:
```python
import jax
import jax.numpy as jnp
from jax import lax
from jax.sharding import PartitionSpec as P

BLENDER_FEATURES = 1024
GROUP_DIM = 128
BLOCK = 128


epsilon = 1e-06


def in_one_piece(arrays, axis, dim, along):
    both = jnp.concatenate(arrays, axis=along)
    result, at, finished = (lax.all_gather(both, axis, axis=dim, tiled=True), 0, [])
    for a in arrays:
        finished.append(lax.slice_in_dim(result, at, at + a.shape[along], axis=along))
        at += a.shape[along]
    return tuple(finished)


def sent_to_all(shard, axis):
    copies = jnp.broadcast_to(shard, (lax.axis_size(axis), *shard.shape))
    return lax.all_to_all(copies, axis, split_axis=0, concat_axis=0, tiled=True)


def laid_out(blocks, dim):
    blocks = jnp.moveaxis(blocks, 0, dim)
    lengths = blocks.shape
    return blocks.reshape(*lengths[:dim], lengths[dim] * lengths[dim + 1], *lengths[dim + 2 :])


def gather_directly(shard, axis, dim):
    blocks = sent_to_all(shard, axis)
    return laid_out(blocks, dim)


def rows_first(arrays, axis, dims):
    turned = [jnp.moveaxis(a, dim, 0) for a, dim in zip(arrays, dims)]
    widths = [t[0].size for t in turned]
    both = jnp.concatenate([t.reshape(-1, w) for t, w in zip(turned, widths)], axis=1)
    result = lax.all_gather(both, axis, axis=0, tiled=True)
    blocks = jnp.split(result, [sum(widths[:k]) for k in range(1, len(widths))], axis=1)
    return tuple(
        (
            jnp.moveaxis(b.reshape(-1, *t.shape[1:]), 0, dim)
            for b, t, dim in zip(blocks, turned, dims)
        )
    )


def of_everyone(shard, axis):
    everything = sent_to_all(shard, axis)
    return jnp.sum(everything, axis=0)


def in_blocks(shard, dim, count):
    before, after = (shard.shape[:dim], shard.shape[dim + 1 :])
    return jnp.moveaxis(shard.reshape(*before, count, -1, *after), dim, 0)


def sent_and_summed(shard, axis, dim):
    blocks = in_blocks(shard, dim, lax.axis_size(axis))
    arrived = lax.all_to_all(blocks, axis, split_axis=0, concat_axis=0, tiled=True)
    return arrived.astype(jnp.float32).sum(axis=0)


def normalize(values, gain):
    return values * lax.rsqrt(jnp.mean(values * values, axis=-1, keepdims=True) + epsilon) * gain


def assembled_entries(pieces, activations):
    segments = in_one_piece((pieces[0], pieces[1]), "fs", 0, 1)
    return tuple(
        (jnp.dot(activations, segment, preferred_element_type=jnp.float32) for segment in segments)
    )


def collect_cols(shard_rows, activations, scales):
    return (
        jnp.dot(
            activations, gather_directly(shard_rows, "fs", 1), preferred_element_type=jnp.float32
        )
        * scales
    )


def on_device(
    skip_stream_entry,
    sequence_blender_factor,
    product_projector,
    product_side_factors,
    placewise_projector,
    placewise_entry_factors,
    placewise_rescale_factor,
    place_cluster_operator,
    placewise_offset_vector,
    blender_result_projector,
    blender_result_factors,
    feedforward_norm_factor,
    switch_projector,
    switch_factors,
    expand_projector,
    expand_factors,
    contract_projector,
    contract_factors,
):
    device_sequence_steps = skip_stream_entry.shape[0]
    tp_index = lax.axis_index("tp")
    own_features = skip_stream_entry.shape[1] // lax.axis_size("tp")
    out_scales = rows_first((blender_result_factors, contract_factors), "fs", (0, 0))
    standardized_stream = normalize(
        skip_stream_entry.astype(jnp.float32), sequence_blender_factor
    ).astype(jnp.bfloat16)
    product_plain, diffuse_plain = assembled_entries(
        (product_projector.astype(jnp.bfloat16), placewise_projector.astype(jnp.bfloat16)),
        standardized_stream,
    )
    product_portion = jax.nn.gelu(product_plain * product_side_factors)
    spread = jax.nn.gelu(diffuse_plain * placewise_entry_factors)
    feature_total = spread.shape[1]
    squares = of_everyone(jnp.sum(spread * spread, axis=1), "tp")
    factor = lax.rsqrt(squares / BLENDER_FEATURES + epsilon)
    spread_normed = (spread * factor[:, None] * placewise_rescale_factor).astype(jnp.bfloat16)
    group_span = min(feature_total, GROUP_DIM)
    group_count = max(1, feature_total // GROUP_DIM)
    first_group = tp_index * feature_total // GROUP_DIM
    causal = jnp.tril(jnp.ones((BLOCK, BLOCK), dtype=bool))
    local_weight = lax.dynamic_slice_in_dim(place_cluster_operator, first_group, group_count, 0)
    local_weight = jnp.where(causal[None], local_weight, jnp.zeros_like(local_weight))
    local_bias = lax.dynamic_slice_in_dim(placewise_offset_vector, first_group, group_count, 0)
    blocks = spread_normed.reshape(device_sequence_steps // BLOCK, BLOCK, group_count, group_span)
    blended_sequence = jnp.einsum(
        "gts,nsgc->ntgc", local_weight, blocks, preferred_element_type=jnp.float32
    )
    blended_sequence = blended_sequence + local_bias.T[None, :, :, None]
    switched_inner = (
        product_portion * blended_sequence.reshape(device_sequence_steps, feature_total)
    ).astype(jnp.bfloat16)
    mix_terms = collect_cols(
        blender_result_projector.astype(jnp.bfloat16), switched_inner, out_scales[0]
    )
    mix_total = sent_and_summed(mix_terms.astype(jnp.bfloat16), "tp", 1)
    own_input = lax.dynamic_slice_in_dim(
        skip_stream_entry, tp_index * own_features, own_features, 1
    )
    stream = (own_input.astype(jnp.float32) + mix_total).astype(jnp.bfloat16)
    stream_whole = gather_directly(stream, "tp", 1)
    ffn_normed = normalize(stream_whole.astype(jnp.float32), feedforward_norm_factor).astype(
        jnp.bfloat16
    )
    gate_raw, up_raw = assembled_entries(
        (switch_projector.astype(jnp.bfloat16), expand_projector.astype(jnp.bfloat16)), ffn_normed
    )
    active = (jax.nn.silu(gate_raw * switch_factors) * (up_raw * expand_factors)).astype(
        jnp.bfloat16
    )
    ffn_terms = collect_cols(contract_projector.astype(jnp.bfloat16), active, out_scales[1])
    ffn_total = sent_and_summed(ffn_terms.astype(jnp.bfloat16), "tp", 1)
    return (stream.astype(jnp.float32) + ffn_total).astype(jnp.bfloat16)


def solution(mesh):
    return jax.shard_map(
        on_device,
        mesh=mesh,
        in_specs=(
            P(("rep", "fs"), None),
            P(),
            P("fs", "tp"),
            P("tp"),
            P("fs", "tp"),
            P("tp"),
            P("tp"),
            P(),
            P(),
            P("tp", "fs"),
            P("fs"),
            P(),
            P("fs", "tp"),
            P("tp"),
            P("fs", "tp"),
            P("tp"),
            P("tp", "fs"),
            P("fs"),
        ),
        out_specs=P(("rep", "fs"), "tp"),
        check_vma=False,
    )
```

profile of v0, /device:TPU:1, one launch (start us, length us, event | category | flops | bytes accessed | tf_op | source)
XLA Modules:
  0.0 719.9 jit_solution(17156163401229525524)
XLA Ops:
  6.5 0.0 copy-start
  6.5 0.0 all-gather.4.cloned.1.call-start
  6.5 0.8 convert_element_type.77
  7.3 0.8 convert_element_type.76
  8.1 0.6 pad_maximum_fusion.1
  8.7 0.0 all-gather.4.cloned.1.call-update
  8.7 1.5 fusion.2
  10.2 0.0 copy-start.8
  10.3 0.0 copy-start.9
  10.3 0.0 copy-start.7
  10.3 0.0 copy-start.1
  10.3 0.0 copy-start.10
  10.3 0.0 copy-start.13
  10.3 217.4 %all-gather.4.cloned.1.call-done = bf16[2048,256]{1,0:T(8,128)(2,1)} async-done(((bf16[64,256]{1,0:T(8,128)(2,1)}), bf16[2048,256]{1,0:T(8,128)(2,1)}) %all-gather.4.cloned.1.call-update) | async-done | bytes 1048592 | tf_op jit(solution)/shard_map/all_gather | solution.py:16
  227.7 2.0 multiply_reduce_fusion.1
  229.7 0.6 broadcast_in_dim.12
  230.3 28.2 %all-to-all-start = ((f32[8,1,256]{2,1,0:T(1,128)}), f32[8,1,256]{2,1,0:T(1,128)S(1)}, u32[]{:S(2)}, u32[]{:S(2)}) async-start(f32[8,1,256]{2,1,0:T(1,128)} %broadcast_in_dim.12), calls=%async_computation | async-start | bytes 16384 | tf_op jit(solution)/shard_map/all_to_all | solution.py:25
  258.4 0.0 copy-done.5
  258.4 4.6 all-to-all-done
  263.1 1.0 broadcast_in_dim.14
  264.0 11.0 %all-to-all-start.1 = ((bf16[32,128,64]{1,2,0:T(8,128)(2,1)}), bf16[32,128,64]{1,2,0:T(8,128)(2,1)S(1)}, u32[]{:S(2)}, u32[]{:S(2)}) async-start(bf16[32,128,64]{1,2,0:T(8,128)(2,1)} %broadcast_in_dim.14), calls=%async_computation.1 | async-start | bytes 1048576 | tf_op jit(solution)/shard_map/all_to_all | solution.py:25
  275.0 0.0 copy-done.8
  275.0 0.0 copy-done.9
  275.0 107.8 %all-gather = f32[32,64,2]{1,2,0:T(2,128)S(1)} all-gather(f32[1,64,2]{1,2,0:T(2,128)S(1)} %maximum_bitcast_fusion), channel_id=1, replica_groups=mesh['rep'=4,'fs'=32,'tp'=8] {'fs'}, dimensions={0}, use_global_device_ids=true | all-gather | bytes 16896 | tf_op jit(solution)/shard_map/all_gather | solution.py:43
  382.9 0.1 reshape.92
  383.0 0.0 copy-done
  383.1 0.0 copy-done.7
  383.1 0.1 multiply_convert_fusion
  383.2 0.9 fusion.25
  384.1 0.0 all-to-all-done.1
  384.1 0.0 copy-done.1
  384.1 0.0 copy-done.10
  384.1 1.9 fusion
  386.1 1.1 copy.42
  387.1 18.6 %all-to-all-start.2 = ((bf16[8,256,256]{2,1,0:T(8,128)(2,1)}), bf16[8,256,256]{2,1,0:T(8,128)(2,1)S(1)}, u32[]{:S(2)}, u32[]{:S(2)}) async-start(bf16[8,256,256]{2,1,0:T(8,128)(2,1)} %bitcast.54), calls=%async_computation.2 | async-start | bytes 2097152 | tf_op jit(solution)/shard_map/all_to_all | solution.py:65
  405.7 15.0 %all-to-all-done.2 = bf16[8,256,256]{2,1,0:T(8,128)(2,1)S(1)} async-done(((bf16[8,256,256]{2,1,0:T(8,128)(2,1)}), bf16[8,256,256]{2,1,0:T(8,128)(2,1)S(1)}, u32[]{:S(2)}, u32[]{:S(2)}) %all-to-all-start.2) | async-done | bytes 1048608 | tf_op jit(solution)/shard_map/all_to_all | solution.py:65
  420.7 0.1 convert_reduce_fusion.1
  420.8 0.0 copy-start.2
  420.9 0.1 copy.34
  421.0 1.1 broadcast_in_dim.15
  422.0 4.4 all-to-all-start.3
  426.5 0.0 copy-done.2
  426.5 0.0 copy-start.3
  426.5 0.0 copy-start.4
  426.5 15.0 %all-to-all-done.3 = bf16[8,256,256]{1,2,0:T(8,128)(2,1)S(1)} async-done(((bf16[8,256,256]{1,2,0:T(8,128)(2,1)}), bf16[8,256,256]{1,2,0:T(8,128)(2,1)S(1)}, u32[]{:S(2)}, u32[]{:S(2)}) %all-to-all-start.3) | async-done | bytes 1048608 | tf_op jit(solution)/shard_map/all_to_all | solution.py:25
  441.5 1.4 broadcast_in_dim.16
  442.9 4.1 all-to-all-start.4
  447.0 0.0 copy-start.11
  447.0 0.0 all-gather.6.cloned.1.call-start
  447.0 0.0 copy-done.3
  447.1 0.0 copy-done.4
  447.1 0.7 pad_maximum_fusion
  447.8 0.0 all-gather.6.cloned.1.call-update
  447.8 0.3 multiply_reduce_fusion
  448.2 1.4 fusion.6
  449.5 213.9 %all-gather.6.cloned.1.call-done = bf16[2048,704]{1,0:T(8,128)(2,1)} async-done(((bf16[64,704]{1,0:T(8,128)(2,1)}), bf16[2048,704]{1,0:T(8,128)(2,1)}) %all-gather.6.cloned.1.call-update) | async-done | bytes 2883600 | tf_op jit(solution)/shard_map/all_gather | solution.py:16
  663.4 0.0 copy-done.11
  663.4 2.5 fusion.11
  665.9 0.0 all-to-all-done.4
  665.9 4.5 fusion.1
  670.4 0.1 copy.41
  670.5 41.7 %all_to_all.31 = bf16[8,256,256]{2,1,0:T(8,128)(2,1)S(1)} all-to-all(bf16[8,256,256]{2,1,0:T(8,128)(2,1)S(1)} %bitcast.55), channel_id=1, replica_groups=mesh['rep'=4,'fs'=32,'tp'=8] {'tp'}, dimensions={0} | all-to-all | bytes 2097152 | tf_op jit(solution)/shard_map/all_to_all | solution.py:65
  712.2 0.1 convert_reduce_fusion
  712.4 0.7 add_convert_fusion
  (19 shorter events, 0.2 us)
Async XLA Ops:
  6.5 376.5 %copy-start = (f32[8,128]{1,0:T(8,128)S(1)}, f32[8,128]{1,0:T(8,128)}, u32[]{:S(2)}) copy-start(f32[8,128]{1,0:T(8,128)} %param.26) | copy-start | bytes 12292
  6.5 221.1 %all-gather.4.cloned.1.call-start = ((), (), s32[]{:S(2)}) async-start(), calls=%async_computation.6 | async-start | bytes 1081344 | tf_op jit(solution)/shard_map/all_gather | solution.py:16
  8.7 249.7 %copy-start.5 = (f32[128,64]{0,1:T(8,128)S(1)}, f32[128,64]{0,1:T(8,128)}, u32[]{:S(2)}) copy-start(f32[128,64]{0,1:T(8,128)} %param.27) | copy-start | bytes 98308
  10.2 264.8 %copy-start.8 = (f32[64]{0:T(128)S(1)}, f32[64]{0:T(128)}, u32[]{:S(2)}) copy-start(f32[64]{0:T(128)} %param.35) | copy-start | bytes 772
  10.3 264.8 %copy-start.9 = (f32[64]{0:T(128)S(1)}, f32[64]{0:T(128)}, u32[]{:S(2)}) copy-start(f32[64]{0:T(128)} %param.28) | copy-start | bytes 772
  10.3 372.8 %copy-start.7 = (f32[128]{0:T(128)S(1)}, f32[128]{0:T(128)}, u32[]{:S(2)}) copy-start(f32[128]{0:T(128)} %param.24) | copy-start | bytes 1540
  10.3 373.8 %copy-start.1 = (bf16[256,2048]{1,0:T(8,128)(2,1)S(1)}, bf16[256,2048]{1,0:T(8,128)(2,1)}, u32[]{:S(2)}) copy-start(bf16[256,2048]{1,0:T(8,128)(2,1)} %param.18) | copy-start | bytes 3145732
  10.3 373.8 %copy-start.10 = (f32[2048]{0:T(1024)S(1)}, f32[2048]{0:T(1024)}, u32[]{:S(2)}) copy-start(f32[2048]{0:T(1024)} %param.19) | copy-start | bytes 24580
  10.3 373.8 %copy-start.13 = (f32[128]{0:T(128)S(1)}, f32[128]{0:T(128)}, u32[]{:S(2)}) copy-start(f32[128]{0:T(128)} %param.21) | copy-start | bytes 1540
  230.3 32.8 %all-to-all-start = ((f32[8,1,256]{2,1,0:T(1,128)}), f32[8,1,256]{2,1,0:T(1,128)S(1)}, u32[]{:S(2)}, u32[]{:S(2)}) async-start(f32[8,1,256]{2,1,0:T(1,128)} %broadcast_in_dim.12), calls=%async_computation | async-start | bytes 16384 | tf_op jit(solution)/shard_map/all_to_all | solution.py:25
  264.0 120.1 %all-to-all-start.1 = ((bf16[32,128,64]{1,2,0:T(8,128)(2,1)}), bf16[32,128,64]{1,2,0:T(8,128)(2,1)S(1)}, u32[]{:S(2)}, u32[]{:S(2)}) async-start(bf16[32,128,64]{1,2,0:T(8,128)(2,1)} %broadcast_in_dim.14), calls=%async_computation.1 | async-start | bytes 1048576 | tf_op jit(solution)/shard_map/all_to_all | solution.py:25
  387.1 33.6 %all-to-all-start.2 = ((bf16[8,256,256]{2,1,0:T(8,128)(2,1)}), bf16[8,256,256]{2,1,0:T(8,128)(2,1)S(1)}, u32[]{:S(2)}, u32[]{:S(2)}) async-start(bf16[8,256,256]{2,1,0:T(8,128)(2,1)} %bitcast.54), calls=%async_computation.2 | async-start | bytes 2097152 | tf_op jit(solution)/shard_map/all_to_all | solution.py:65
  420.8 5.6 copy-start.2
  422.0 19.4 %all-to-all-start.3 = ((bf16[8,256,256]{1,2,0:T(8,128)(2,1)}), bf16[8,256,256]{1,2,0:T(8,128)(2,1)S(1)}, u32[]{:S(2)}, u32[]{:S(2)}) async-start(bf16[8,256,256]{1,2,0:T(8,128)(2,1)} %broadcast_in_dim.15), calls=%async_computation.3 | async-start | bytes 2097152 | tf_op jit(solution)/shard_map/all_to_all | solution.py:25
  426.5 20.6 %copy-start.3 = (f32[64,352]{1,0:T(8,128)S(1)}, f32[64,352]{1,0:T(8,128)}, u32[]{:S(2)}) copy-start(f32[64,352]{1,0:T(8,128)} %param.32) | copy-start | bytes 270340
  426.5 20.6 %copy-start.4 = (f32[64,352]{1,0:T(8,128)S(1)}, f32[64,352]{1,0:T(8,128)}, u32[]{:S(2)}) copy-start(f32[64,352]{1,0:T(8,128)} %param.30) | copy-start | bytes 270340
  442.9 5.3 copy-start.6
  442.9 223.0 %all-to-all-start.4 = ((bf16[32,352,64]{1,2,0:T(8,128)(2,1)}), bf16[32,352,64]{1,2,0:T(8,128)(2,1)S(1)}, u32[]{:S(2)}, u32[]{:S(2)}) async-start(bf16[32,352,64]{1,2,0:T(8,128)(2,1)} %broadcast_in_dim.16), calls=%async_computation.4 | async-start | bytes 3145728 | tf_op jit(solution)/shard_map/all_to_all | solution.py:25
  447.0 216.4 %copy-start.11 = (f32[352]{0:T(512)S(1)}, f32[352]{0:T(512)}, u32[]{:S(2)}) copy-start(f32[352]{0:T(512)} %param.31) | copy-start | bytes 4228
  447.0 216.4 %all-gather.6.cloned.1.call-start = ((), (), s32[]{:S(2)}) async-start(), calls=%async_computation.7 | async-start | bytes 3244032 | tf_op jit(solution)/shard_map/all_gather | solution.py:16
  449.5 216.4 %copy-start.12 = (f32[352]{0:T(512)S(1)}, f32[352]{0:T(512)}, u32[]{:S(2)}) copy-start(f32[352]{0:T(512)} %param.33) | copy-start | bytes 4228
Sparse Core Ops, SparseCore 0:
  10.0 217.6 all-gather.3
  450.5 212.8 all-gather.5
where the time goes:
time: 721 us; the launch traced here: 720 us
  waiting for transfers between devices  466 us (65%)
  blocking collectives  150 us (21%)
  starting transfers between devices  66.3 us (9%)
  between operations  13.7 us (2%)
  matrix products  11.8 us (2%)
  other arithmetic  7.28 us (1%)
    all_gather x2, waiting for transfers between devices, in_one_piece(): lax.all_gather(both, axis, axis=dim, tiled=True)  431 us
    all_gather x1, blocking collectives, rows_first(): result = lax.all_gather(both, axis, axis=0, tiled=True)  108 us
    all_to_all x4, starting transfers between devices, sent_to_all(): return lax.all_to_all(copies, axis, split_axis=0, concat_axis=0, tiled=True)  47.7 us
    all_to_all x1, blocking collectives, sent_and_summed(): lax.all_to_all(blocks, axis, split_axis=0, concat_axis=0, tiled=True)  41.7 us
    all_to_all x4, waiting for transfers between devices, sent_to_all(): return lax.all_to_all(copies, axis, split_axis=0, concat_axis=0, tiled=True)  19.6 us
    all_to_all x1, starting transfers between devices, sent_and_summed(): lax.all_to_all(blocks, axis, split_axis=0, concat_axis=0, tiled=True)  18.6 us
    all_to_all x1, waiting for transfers between devices, sent_and_summed(): lax.all_to_all(blocks, axis, split_axis=0, concat_axis=0, tiled=True)  15 us
  transfers between devices with their start and end apart: 7, of which 5 were waited for; matrix products, arithmetic and copies ran while one was open for 1% of the time, Pallas kernels for 0%

commit v1 on v0

v1 whole, which is shorter than its diff:
```python
import functools

import jax
import jax.numpy as jnp
from jax import lax
from jax.experimental import pallas as pl
from jax.experimental.pallas import tpu as pltpu
from jax.sharding import PartitionSpec as P

EPS = 1e-06
F32 = jnp.float32
BF16 = jnp.bfloat16
MESH = pl.DeviceIdType.MESH

TOK = 256
BLOCK = 128
DIM = 2048
CH = 1024
HID = 352
NY, NZ, NX, NTP, NREP = 4, 8, 4, 8, 4

R_PROD, R_PLACE, R_BLEND, R_SE, R_CON, R_ALL = 0, 64, 128, 192, 576, 768

RING4 = {1: 0, 2: 1, 3: 2, 4: 3, -1: 0, -2: -1, -3: -2}
RING3 = {1: 0, 2: 1, 3: 2, -1: 0, -2: -1, -3: -2, -4: -3}
JUMP4 = {1: 0, 2: 0, 3: 2, 4: 2, -1: 0, -2: 0, -3: -2}
JUMP3 = {1: 0, 2: 0, 3: 2, -1: 0, -2: 0, -3: -2, -4: -2}
FAR4 = {1: 0, 2: 0, 3: 0, 4: 0, -1: 0, -2: 0, -3: 0}
FAR3 = {1: 0, 2: 0, 3: 0, -1: 0, -2: 0, -3: 0, -4: 0}
YUP = {1: 0, -1: 0, 2: 1}
YDN = {1: 0, -1: 0, -2: -1}
YUP2 = {1: 0, -1: 0, 2: 0}
YDN2 = {1: 0, -1: 0, -2: 0}

STREAMS = (
    (R_PROD, 64, "z", JUMP4, YUP, 0.0),
    (R_PLACE, 64, "y", JUMP3, YDN, 0.0),
    (R_BLEND, 64, "y", RING4, YDN, 0.0),
    (R_SE, 128, "z", RING3, YUP, 4.0),
    (R_SE + 128, 128, "z", RING4, YDN, 8.0),
    (R_SE + 256, 128, "z", RING3, YUP, 10.0),
    (R_CON, 192, "y", RING4, YDN, 12.0),
)
IN, BLEND, SE, CON = (0, 1), (2,), (3, 4, 5), (6,)


def order_of(tree):
    return sorted(tree, key=lambda d: (abs(d), -d))


def arrivals_of(stream):
    first, zt, yt = stream[2:5]
    out = {}
    if first == "z":
        for dz in order_of(zt):
            out[(dz, 0)] = ((zt[dz], 0), "z", dz - zt[dz])
        for dz in [0, *order_of(zt)]:
            for dy in order_of(yt):
                out[(dz, dy)] = ((dz, yt[dy]), "y", dy - yt[dy])
    else:
        for dy in order_of(yt):
            out[(0, dy)] = ((0, yt[dy]), "y", dy - yt[dy])
        for dy in [0, *order_of(yt)]:
            for dz in order_of(zt):
                out[(dz, dy)] = ((zt[dz], dy), "z", dz - zt[dz])
    return out


class Plan:
    def __init__(self):
        self.tasks = {}
        self.copies = {}

    def copy(self, key, link, size, hops):
        self.copies[key] = len(self.copies)
        return (key, link, size, hops)

    def task(self, key, deps, dur, sends=(), rank=1, begin=0.0):
        self.tasks[key] = (tuple(deps), dur, tuple(sends), rank, begin)

    def order(self):
        t, arrived, free, done, seq = 0.0, {}, {}, {}, []
        left = dict(self.tasks)
        while left:
            best, when = None, None
            for key, (deps, _, _, rank, begin) in left.items():
                ready = begin
                for d in deps:
                    at = done.get(d) if d in self.tasks else arrived.get(d)
                    if at is None:
                        ready = None
                        break
                    ready = max(ready, at)
                if ready is None:
                    continue
                mark = (max(ready, t), rank, ready)
                if when is None or mark < when:
                    best, when = key, mark
            deps, dur, sends, *_ = left.pop(best)
            t = max(t, when[0]) + dur
            done[best] = t
            for key, link, size, hops in sends:
                rate = 650e3 if link == "d2d" else 46.6e3
                begin = max(free.get(link, 0.0), t)
                wire = size * max(hops, 1) / rate
                free[link] = begin + wire
                arrived[key] = begin + wire + (1.0 if link == "d2d" else 1.4 + 0.75 * hops)
            seq.append((best, t))
        return seq


def make_plan():
    plan = Plan()
    stream_tasks = {}
    plan.task("pack1", [], 2.0)
    plan.task("pack2", ["pack1"], 0.5, (), 2)
    plan.task("pack3", ["pack1"], 0.5, (), 3)
    for s, stream in enumerate(STREAMS):
        arr = arrivals_of(stream)
        sends = {}
        for a, (parent, axis, step) in arr.items():
            key = ("w", s, *a)
            link = axis + ("+" if step > 0 else "-")
            cp = plan.copy(key, link, stream[1] * 256, abs(step))
            sends.setdefault(parent, []).append(cp)
        pack = "pack1" if s in IN + BLEND else "pack2" if s in SE else "pack3"
        plan.task(("go", s), [pack], 0.03, sends[(0, 0)], 0, stream[5])
        for a in arr:
            key = ("w", s, *a)
            plan.task(("recv", s, *a), [key, ("go", s)], 0.03, sends.get(a, ()), 0)
        stream_tasks[s] = [("recv", s, *a) for a in arr]
    def whole(which):
        return [t for s in which for t in stream_tasks[s]]

    plan.task("norm", ["pack1"], 1.5, (), 2)
    sq = [plan.copy(("sq", k), "d2d" if k == 4 else "q", 1024, 1) for k in range(1, NTP)]
    plan.task("in", ["norm", *whole(IN)], 1.5, sq, 2)
    plan.task("mask", ["pack1"], 0.2, (), 3)
    plan.task("mixed", ["in", "mask", *[("sq", k) for k in range(1, NTP)]], 0.8, (), 1)

    def scatter(w, deps, dur):
        last = deps
        for k in (2, 1, 3, 0):
            cp = plan.copy(("p", w, k), "d2d", 131072, 1)
            plan.task(("part", w, k), last, dur, (cp,), 1)
            last = [("part", w, k)]
        for k in (2, 1, 3, 0):
            cps = ()
            if k:
                cps = (plan.copy(("c", w, k), "x-" if k == 3 else "x+", 131072, 2 if k == 2 else 1),)
            plan.task(("sum", w, k), [*last, ("p", w, k)], dur + 0.1, cps, 1)
            last = [("sum", w, k)]
        return [*last, *[("c", w, k) for k in (1, 2, 3)]]

    after = scatter(0, ["mixed", *whole(BLEND)], 0.2)
    ag = [plan.copy(("ap", 0), "d2d", 131072, 1)]
    for k in (2, 1, 3):
        ag.append(plan.copy(("ac", k), "x-" if k == 3 else "x+", 131072, 2 if k == 2 else 1))
    plan.task("stream", after, 0.3, ag, 1)
    for k in (1, 3, 2):
        plan.task(("pass", k), [("ac", k), "stream"], 0.03, (plan.copy(("ap", k), "d2d", 131072, 1),), 0)
    got = [("pass", k) for k in (1, 2, 3)] + [("ap", k) for k in range(4)]
    plan.task("norm2", ["stream", *got], 1.5, (), 1)
    plan.task("hidden", ["norm2", *whole(SE)], 3.0, (), 1)
    after = scatter(1, ["hidden", *whole(CON)], 0.3)
    plan.task("out", after, 0.3, (), 1)
    return plan


def kernel(
    plan,
    seq,
    x_ref,
    gain1_ref,
    wprod_ref,
    sprod_ref,
    wplace_ref,
    splace_ref,
    gains_ref,
    op_ref,
    bias_ref,
    wblend_ref,
    sblend_ref,
    gain2_ref,
    wsw_ref,
    ssw_ref,
    wex_ref,
    sex_ref,
    wcon_ref,
    scon_ref,
    out_ref,
    g,
    normed,
    carrier,
    spread,
    sqbuf,
    opm,
    gated,
    active,
    psend,
    precv,
    csend,
    crecv,
    own,
    sbuf,
    scale,
    send_sem,
    recv_sem,
):
    rep, fs, tp = lax.axis_index("rep"), lax.axis_index("fs"), lax.axis_index("tp")
    zl, y = fs // NY, lax.rem(fs, NY)
    x, core = tp // 2, lax.rem(tp, 2)
    z = rep * NZ + zl

    def at_z(d):
        zz = lax.rem(z + d + NREP * NZ, NREP * NZ)
        return {"rep": zz // NZ, "fs": lax.rem(zz, NZ) * NY + y}

    def at_y(d):
        return {"fs": zl * NY + lax.rem(y + d + NY, NY)}

    def at_tp(k):
        return {"tp": lax.rem(tp + k + NTP, NTP)}

    def at_x(k):
        return {"tp": lax.rem(x + k + NX, NX) * 2 + core}

    partner = {"tp": x * 2 + 1 - core}

    def slot(a):
        return lax.rem(zl - a[0] + NZ, NZ) * NY + lax.rem(y - a[1] + NY, NY)

    pending = []

    def send(key, src, dst, dev):
        i = plan.copies[key]
        cp = pltpu.make_async_remote_copy(
            src_ref=src, dst_ref=dst, send_sem=send_sem.at[i], recv_sem=recv_sem.at[i],
            device_id=dev, device_id_type=MESH,
        )
        cp.start()
        pending.append(cp)

    def arrive(key, dst, dev):
        i = plan.copies[key]
        pltpu.make_async_remote_copy(
            src_ref=dst, dst_ref=dst, send_sem=send_sem.at[i], recv_sem=recv_sem.at[i],
            device_id=dev, device_id_type=MESH,
        ).wait_recv()

    arrs = [arrivals_of(s) for s in STREAMS]

    def block(s, a):
        return g.at[slot(a), pl.ds(STREAMS[s][0], STREAMS[s][1])]

    def forward(s, a):
        for b, (parent, axis, step) in arrs[s].items():
            if parent == a:
                send(("w", s, *b), block(s, a), block(s, a), at_z(step) if axis == "z" else at_y(step))

    zs = sorted({e * v[2] for a in arrs for v in a.values() if v[1] == "z" for e in (1, -1)})
    ys = sorted({(e * v[2]) % NY for a in arrs for v in a.values() if v[1] == "y" for e in (1, -1)})
    greet = [at_z(d) for d in zs] + [at_y(d) for d in ys] + [at_tp(k) for k in range(1, NTP)]
    barrier = pltpu.get_barrier_semaphore()
    for dev in greet:
        pl.semaphore_signal(barrier, inc=1, device_id=dev, device_id_type=MESH)

    def pack1():
        g[fs, R_PROD : R_PROD + 64, :] = wprod_ref[...].astype(BF16)
        g[fs, R_PLACE : R_PLACE + 64, :] = wplace_ref[...].astype(BF16)
        wb = (wblend_ref[...].astype(BF16).astype(F32) * sblend_ref[...]).T
        g[fs, R_BLEND : R_BLEND + 64, :] = wb.astype(BF16)
        pl.semaphore_wait(barrier, len(greet))

    def pack2():
        for i, w in ((0, wsw_ref), (2, wex_ref)):
            for j in (0, 1):
                g[fs, R_SE + 64 * (i + j) : R_SE + 64 * (i + j + 1), :] = w[:, 128 * j : 128 * (j + 1)].astype(BF16)
        zero = jnp.zeros((64, 128), BF16)
        for i, w in ((4, wsw_ref), (5, wex_ref)):
            g[fs, R_SE + 64 * i : R_SE + 64 * (i + 1), :] = zero
            g[fs, R_SE + 64 * i : R_SE + 64 * (i + 1), 0:96] = w[:, 256:352].astype(BF16)
        scale[...] = jnp.zeros_like(scale)
        scale[0:1, 0:HID] = ssw_ref[...]
        scale[1:2, 0:HID] = sex_ref[...]

    def pack3():
        wc = (wcon_ref[...].astype(BF16).astype(F32) * scon_ref[...]).T.astype(BF16)
        g[fs, R_CON : R_CON + 64, :] = wc[:, 0:128]
        g[fs, R_CON + 64 : R_CON + 128, :] = wc[:, 128:256]
        g[fs, R_CON + 128 : R_CON + 192, :] = jnp.zeros((64, 128), BF16)
        g[fs, R_CON + 128 : R_CON + 192, 0:96] = wc[:, 256:352]

    def go(s):
        forward(s, (0, 0))

    def recv(s, dz, dy):
        _, axis, step = arrs[s][(dz, dy)]
        arrive(("w", s, dz, dy), block(s, (dz, dy)), at_z(-step) if axis == "z" else at_y(-step))
        forward(s, (dz, dy))

    def tile(row):
        return g[:, row : row + 64, :].reshape(DIM, 128)

    def norm():
        v = x_ref[...].astype(F32)
        r = lax.rsqrt(jnp.mean(v * v, axis=-1, keepdims=True) + EPS)
        normed[...] = (v * r * gain1_ref[...]).astype(BF16)

    def enter():
        w = jnp.concatenate([tile(R_PROD), tile(R_PLACE)], axis=1)
        h = jnp.dot(normed[...], w, preferred_element_type=F32)
        sp = jax.nn.gelu(h[:, 128:256] * splace_ref[...])
        spread[...] = sp
        sqbuf[tp] = jnp.sum((sp * sp).T, axis=0, keepdims=True)
        for k in range(1, NTP):
            send(("sq", k), sqbuf.at[tp], sqbuf.at[tp], at_tp(k))
        carrier[...] = jax.nn.gelu(h[:, 0:128] * sprod_ref[...])

    def mask():
        t = lax.broadcasted_iota(jnp.int32, (BLOCK, BLOCK), 0)
        s = lax.broadcasted_iota(jnp.int32, (BLOCK, BLOCK), 1)
        opm[...] = jnp.where(t >= s, op_ref[tp].astype(F32), 0.0).astype(BF16)

    def mixed():
        for k in range(1, NTP):
            src = lax.rem(tp - k + NTP, NTP)
            arrive(("sq", k), sqbuf.at[src], at_tp(-k))
        total = jnp.sum(sqbuf[...], axis=0)
        r = lax.rsqrt(total / CH + EPS)
        r = jnp.broadcast_to(r, (128, TOK)).T
        sn = (spread[...] * r * gains_ref[...]).astype(BF16)
        bias = jnp.broadcast_to(bias_ref[pl.ds(tp, 1), :], (BLOCK, BLOCK)).T
        w = opm[...]
        for n in range(TOK // BLOCK):
            rows = slice(n * BLOCK, (n + 1) * BLOCK)
            m = jnp.dot(w, sn[rows], preferred_element_type=F32) + bias
            gated[rows, :] = (carrier[rows, :] * m).astype(BF16)

    nt = (((1,), (1,)), ((), ()))

    def product(w, d):
        if w == 0:
            b = g[pl.ds(4 * d, 4), R_BLEND : R_BLEND + 64, :].reshape(256, 128)
            return lax.dot_general(gated[...], b, nt, preferred_element_type=F32)
        cols = [g[pl.ds(4 * d, 4), R_CON + 64 * j : R_CON + 64 * (j + 1), :].reshape(256, 128) for j in range(3)]
        return lax.dot_general(active[...], jnp.concatenate(cols, axis=1), nt, preferred_element_type=F32)

    def chip(k):
        return lax.rem(x + k, NX) * 2

    def part(w, k):
        psend[w, k] = product(w, chip(k) + 1 - core).astype(BF16)
        send(("p", w, k), psend.at[w, k], precv.at[w, k], partner)

    def add(w, k):
        v = product(w, chip(k) + core)
        arrive(("p", w, k), precv.at[w, k], partner)
        v = v + precv[w, k].astype(F32)
        if k == 0:
            own[...] = v
        else:
            csend[w, k - 1] = v.astype(BF16)
            send(("c", w, k), csend.at[w, k - 1], crecv.at[w, k - 1], at_x(k))

    def total(w):
        v = own[...]
        for k in (1, 2, 3):
            arrive(("c", w, k), crecv.at[w, k - 1], at_x(-k))
            v = v + crecv[w, k - 1].astype(F32)
        return v

    def stream():
        mine = x_ref[:, pl.ds(pl.multiple_of(tp * 256, 256), 256)].astype(F32)
        sbuf[tp] = (mine + total(0)).astype(BF16)
        for k in (2, 1, 3):
            send(("ac", k), sbuf.at[tp], sbuf.at[tp], at_x(k))
        send(("ap", 0), sbuf.at[tp], sbuf.at[tp], partner)

    def relay(k):
        d = lax.rem(x - k + NX, NX) * 2 + core
        arrive(("ac", k), sbuf.at[d], at_x(-k))
        send(("ap", k), sbuf.at[d], sbuf.at[d], partner)

    def norm2():
        for k in range(4):
            d = lax.rem(x - k + NX, NX) * 2 + 1 - core
            arrive(("ap", k), sbuf.at[d], partner)
        sq = jnp.zeros((TOK, 256), F32)
        for d in range(NTP):
            v = sbuf[d].astype(F32)
            sq = sq + v * v
        r = lax.rsqrt(jnp.sum(sq, axis=-1, keepdims=True) / DIM + EPS)
        for d in range(NTP):
            cols = slice(256 * d, 256 * (d + 1))
            normed[:, cols] = (sbuf[d].astype(F32) * r * gain2_ref[:, cols]).astype(BF16)

    def hidden():
        for j, (a, b) in enumerate(((0, 2), (1, 3), (4, 5))):
            w = jnp.concatenate([tile(R_SE + 64 * a), tile(R_SE + 64 * b)], axis=1)
            h = jnp.dot(normed[...], w, preferred_element_type=F32)
            cols = slice(128 * j, 128 * (j + 1))
            gate = h[:, 0:128] * scale[0:1, cols]
            up = h[:, 128:256] * scale[1:2, cols]
            active[:, cols] = (gate / (1.0 + jnp.exp(-gate)) * up).astype(BF16)

    def out():
        out_ref[...] = (sbuf[tp].astype(F32) + total(1)).astype(BF16)

    run = {
        "pack1": pack1, "pack2": pack2, "pack3": pack3, "go": go, "norm": norm, "in": enter, "mask": mask, "mixed": mixed, "stream": stream,
        "norm2": norm2, "hidden": hidden, "out": out, "recv": recv, "part": part, "sum": add, "pass": relay,
    }
    for key, _ in seq:
        if isinstance(key, tuple):
            run[key[0]](*key[1:])
        else:
            run[key]()
    for cp in pending:
        cp.wait_send()


def on_device(*args):
    plan = make_plan()
    seq = plan.order()
    n = len(plan.copies)
    args = [a.reshape(1, -1) if a.ndim == 1 else a for a in args]
    return pl.pallas_call(
        functools.partial(kernel, plan, seq),
        out_shape=jax.ShapeDtypeStruct((TOK, 256), BF16),
        in_specs=[pl.BlockSpec(memory_space=pltpu.VMEM)] * len(args),
        out_specs=pl.BlockSpec(memory_space=pltpu.VMEM),
        scratch_shapes=[
            pltpu.VMEM((NY * NZ, R_ALL, 128), BF16),
            pltpu.VMEM((TOK, DIM), BF16),
            pltpu.VMEM((TOK, 128), F32),
            pltpu.VMEM((TOK, 128), F32),
            pltpu.VMEM((NTP, 1, TOK), F32),
            pltpu.VMEM((BLOCK, BLOCK), BF16),
            pltpu.VMEM((TOK, 128), BF16),
            pltpu.VMEM((TOK, 384), BF16),
            pltpu.VMEM((2, 4, TOK, 256), BF16),
            pltpu.VMEM((2, 4, TOK, 256), BF16),
            pltpu.VMEM((2, 3, TOK, 256), BF16),
            pltpu.VMEM((2, 3, TOK, 256), BF16),
            pltpu.VMEM((TOK, 256), F32),
            pltpu.VMEM((NTP, TOK, 256), BF16),
            pltpu.VMEM((8, 384), F32),
            pltpu.SemaphoreType.DMA((n,)),
            pltpu.SemaphoreType.DMA((n,)),
        ],
        compiler_params=pltpu.CompilerParams(
            collective_id=0, has_side_effects=True, vmem_limit_bytes=48 * 1024 * 1024
        ),
        name="layer",
    )(*args)


def solution(mesh):
    return jax.shard_map(
        on_device,
        mesh=mesh,
        in_specs=(
            P(("rep", "fs"), None),
            P(),
            P("fs", "tp"),
            P("tp"),
            P("fs", "tp"),
            P("tp"),
            P("tp"),
            P(),
            P(),
            P("tp", "fs"),
            P("fs"),
            P(),
            P("fs", "tp"),
            P("tp"),
            P("fs", "tp"),
            P("tp"),
            P("tp", "fs"),
            P("fs"),
        ),
        out_specs=P(("rep", "fs"), "tp"),
        check_vma=False,
    )
```

time: 721 us -> 102 us (0.14)
  waiting for transfers between devices: 466 us -> 0 us
  blocking collectives: 150 us -> 0 us
  Pallas kernels: 0 us -> 90.3 us
  starting transfers between devices: 66.3 us -> 0 us
  between operations: 13.7 us -> 0.09 us
  matrix products: 11.8 us -> 0 us
  other arithmetic: 7.28 us -> 0 us
    all_gather x2 -> x0, waiting for transfers between devices: 431 us -> none  [in_one_piece(): lax.all_gather(both, axis, axis=dim, tiled=True)]
    all_gather x1 -> x0, blocking collectives: 108 us -> none  [rows_first(): result = lax.all_gather(both, axis, axis=0, tiled=True)]
    pallas_call x0 -> x1, Pallas kernels: none -> 90.3 us  [on_device(): pl.pallas_call(functools.partial(kernel, plan, seq), out_shape=jax.ShapeD...]
    all_to_all x5 -> x0, starting transfers between devices: 66.2 us -> none  [the longest x4 47.7 us: sent_to_all(): return lax.all_to_all(copies, axis, split_axis=0, concat_axis=0, tiled=True)]
    all_to_all x1 -> x0, blocking collectives: 41.7 us -> none  [sent_and_summed(): lax.all_to_all(blocks, axis, split_axis=0, concat_axis=0, tiled=True)]
    all_to_all x5 -> x0, waiting for transfers between devices: 34.6 us -> none  [the longest x4 19.6 us: sent_to_all(): return lax.all_to_all(copies, axis, split_axis=0, concat_axis=0, tiled=True)]
    dot_general x5 -> x0, matrix products: 11.8 us -> none  [the longest x2 6.44 us: collect_cols(): jnp.dot(activations, gather_directly(shard_rows, 'fs', 1), preferred_elem...]
    unnamed x29 -> x31, local copies, waits for them, and re-layouts: 0.17 us -> 10.1 us
  transfers between devices with their start and end apart: 7 -> 0, of which waited for: 5 -> 0; matrix products, arithmetic and copies ran while one was open for 1% -> 0% of each run, Pallas kernels for 0% -> 0%
where the time goes in v1:
time: 102 us
  Pallas kernels  90.3 us (89%)
  local copies, waits for them, and re-layouts  11.5 us (11%)
    pallas_call x1, Pallas kernels, on_device(): pl.pallas_call(functools.partial(kernel, plan, seq), out_shape=jax.ShapeD...  90.3 us
    unnamed x31, local copies, waits for them, and re-layouts  10.1 us

profile of v1, /device:TPU:1, one launch (start us, length us, event | category | flops | bytes accessed | tf_op | source)
XLA Modules:
  0.0 101.9 jit_solution(2611698605684533963)
XLA Ops:
  0.0 0.0 copy-start.1
  0.0 0.7 reshape.33.ssw_ref
  0.7 0.7 reshape.34.sex_ref
  1.4 0.8 copy.19.wblend_ref
  2.3 0.0 copy-start.2
  2.3 0.0 copy-start.4
  2.3 0.0 copy-start.8
  2.3 1.1 %copy.20.wcon_ref = f32[352,64]{1,0:T(8,128)S(1)} copy(f32[352,64]{0,1:T(8,128)} %param.34) | data formatting | bytes 180224 | tf_op args[16]
  3.4 0.0 copy-done.1
  3.4 0.0 copy-done.2
  3.4 0.0 copy-done.4
  3.4 0.0 copy-done.8
  3.4 0.0 copy-start
  3.4 1.2 %copy-done = bf16[256,2048]{1,0:T(8,128)(2,1)S(1)} copy-done((bf16[256,2048]{1,0:T(8,128)(2,1)S(1)}, bf16[256,2048]{1,0:T(8,128)(2,1)}, u32[]{:S(2)}) %copy-start) | copy-done | bytes 1048600
  4.6 0.0 copy-start.3
  4.6 0.9 copy-done.3
  5.5 0.0 copy-start.5
  5.5 0.8 copy-done.5
  6.3 0.0 copy-start.6
  6.3 0.7 copy-done.6
  7.0 0.0 copy-start.7
  7.0 0.7 copy-done.7
  7.7 0.0 copy-start.9
  7.7 0.7 copy-done.9
  8.3 0.0 copy-start.10
  8.3 0.7 copy-done.10
  9.0 0.0 copy-start.11
  9.0 0.7 copy-done.11
  9.6 0.0 copy-start.12
  9.6 0.7 copy-done.12
  10.3 0.0 copy-start.13
  10.3 0.7 copy-done.13
  11.0 90.3 %layer.1 = bf16[256,256]{1,0:T(8,128)(2,1)S(1)} custom-call(bf16[256,2048]{1,0:T(8,128)(2,1)S(1)} %copy-done, f32[1,2048]{1,0:T(1,128)S(1)} %bitcast.7, f32[64,128]{1,0:T(8,128)S(1)} %copy-done.4, f32[1,128]{1,0:T(1,128)S(1)} %bitcast.9, f32[64,128]{1,0:T(8,128)S(1)} %copy-done.5, f32[1,128]{1,0:T(1,128)S(1)} %bitcast.10, f32[1,128]{1,0:T(1,128)S(1)} %bitcast.11, ...), custom_call_target="tpu_custom_call" | custom-call | tf_op jit(solution)/shard_map/layer/pallas_call | solution.py:428
  101.3 0.7 copy.22
Async XLA Ops:
  0.0 3.4 %copy-start.1 = (bf16[8,128,128]{2,1,0:T(8,128)(2,1)S(1)}, bf16[8,128,128]{2,1,0:T(8,128)(2,1)}, u32[]{:S(2)}) copy-start(bf16[8,128,128]{2,1,0:T(8,128)(2,1)} %op_ref.1) | copy-start | bytes 786436
  2.3 1.1 %copy-start.2 = (f32[64,352]{1,0:T(8,128)S(1)}, f32[64,352]{1,0:T(8,128)}, u32[]{:S(2)}) copy-start(f32[64,352]{1,0:T(8,128)} %wsw_ref.1) | copy-start | bytes 270340
  2.3 1.1 %copy-start.4 = (f32[64,128]{1,0:T(8,128)S(1)}, f32[64,128]{1,0:T(8,128)}, u32[]{:S(2)}) copy-start(f32[64,128]{1,0:T(8,128)} %wprod_ref.1) | copy-start | bytes 98308
  2.3 1.1 %copy-start.8 = (f32[8,128]{1,0:T(8,128)S(1)}, f32[8,128]{1,0:T(8,128)}, u32[]{:S(2)}) copy-start(f32[8,128]{1,0:T(8,128)} %bias_ref.1) | copy-start | bytes 12292
  3.4 1.2 %copy-start = (bf16[256,2048]{1,0:T(8,128)(2,1)S(1)}, bf16[256,2048]{1,0:T(8,128)(2,1)}, u32[]{:S(2)}) copy-start(bf16[256,2048]{1,0:T(8,128)(2,1)} %x_ref.1) | copy-start | bytes 3145732
  4.6 0.9 copy-start.3
  5.5 0.8 copy-start.5
  6.3 0.7 copy-start.6
  7.0 0.7 copy-start.7
  7.7 0.7 copy-start.9
  8.3 0.7 copy-start.10
  9.0 0.7 copy-start.11
  9.6 0.7 copy-start.12
  10.3 0.7 copy-start.13

commit v2 on v1

v2 whole, which is shorter than its diff:
```python
import functools

import jax
import jax.numpy as jnp
from jax import lax
from jax.experimental import pallas as pl
from jax.experimental.pallas import tpu as pltpu
from jax.sharding import PartitionSpec as P

EPS = 1e-06
F32 = jnp.float32
BF16 = jnp.bfloat16
MESH = pl.DeviceIdType.MESH

TOK = 256
BLOCK = 128
DIM = 2048
CH = 1024
HID = 352
NY, NZ, NX, NTP, NREP = 4, 8, 4, 8, 4

R_PROD, R_PLACE, R_BLEND, R_SE, R_CON, R_ALL = 0, 64, 128, 192, 576, 768

RING4 = {1: 0, 2: 1, 3: 2, 4: 3, -1: 0, -2: -1, -3: -2}
RING3 = {1: 0, 2: 1, 3: 2, -1: 0, -2: -1, -3: -2, -4: -3}
JUMP4 = {1: 0, 2: 0, 3: 2, 4: 2, -1: 0, -2: 0, -3: -2}
JUMP3 = {1: 0, 2: 0, 3: 2, -1: 0, -2: 0, -3: -2, -4: -2}
FAR4 = {1: 0, 2: 0, 3: 0, 4: 0, -1: 0, -2: 0, -3: 0}
FAR3 = {1: 0, 2: 0, 3: 0, -1: 0, -2: 0, -3: 0, -4: 0}
YUP = {1: 0, -1: 0, 2: 1}
YDN = {1: 0, -1: 0, -2: -1}
YUP2 = {1: 0, -1: 0, 2: 0}
YDN2 = {1: 0, -1: 0, -2: 0}

KINDS = ("w", "sq", "p", "c", "ac", "ap")
NAMES = (
    "x", "gain1", "wprod", "sprod", "wplace", "splace", "gains", "op", "bias",
    "wblend", "sblend", "gain2", "wsw", "ssw", "wex", "sex", "wcon", "scon",
)
LOADS = (
    "wprod", "wplace", "wblend", "sblend", "wsw", "wex", "wcon", "scon", "x", "gain1", "sprod", "splace",
    "op", "gains", "bias", "ssw", "sex", "gain2",
)

STREAMS = (
    (0, 64, "z", JUMP4, YDN, 0.0, 0.0),
    (64, 64, "z", JUMP3, YUP, 0.0, 0.0),
    (128, 64, "z", JUMP3, YDN, 2.5, 0.0),
    (192, 128, "z", RING4, YUP, 12.2, 1.0),
    (320, 128, "z", JUMP3, YDN, 13.6, 1.0),
    (448, 128, "y", RING3, YUP, 0, 1.0),
    (576, 192, "y", RING4, YUP, 13.2, 1.0),
)
IN, BLEND, SE, CON = (0, 1), (2,), (3, 4, 5), (6,)


def order_of(tree):
    return sorted(tree, key=lambda d: (abs(d), -d))


def arrivals_of(stream):
    first, zt, yt = stream[2:5]
    out = {}
    if first == "z":
        for dz in order_of(zt):
            out[(dz, 0)] = ((zt[dz], 0), "z", dz - zt[dz])
        for dz in [0, *order_of(zt)]:
            for dy in order_of(yt):
                out[(dz, dy)] = ((dz, yt[dy]), "y", dy - yt[dy])
    else:
        for dy in order_of(yt):
            out[(0, dy)] = ((0, yt[dy]), "y", dy - yt[dy])
        for dy in [0, *order_of(yt)]:
            for dz in order_of(zt):
                out[(dz, dy)] = ((zt[dz], dy), "z", dz - zt[dz])
    return out


def leaves_of(arrivals):
    parents = {v[0] for v in arrivals.values()}
    return [a for a in arrivals if a not in parents]


class Plan:
    def __init__(self):
        self.tasks = {}
        self.copies = {}
        self.groups = {}

    def copy(self, key, link, size, hops, group=None):
        self.copies[key] = self.groups.setdefault(group or key, len(self.groups))
        return (key, link, size, hops)

    def task(self, key, deps, dur, sends=(), rank=1, begin=0.0, slack=0.0):
        self.tasks[key] = (tuple(deps), dur, tuple(sends), rank, begin, slack)

    def order(self):
        t, arrived, free, done, seq = 0.0, {}, {}, {}, []
        waits = {k: sum(1 for _ in v[0]) for k, v in self.tasks.items()}
        users, ready, open_ = {}, {k: v[4] for k, v in self.tasks.items()}, set()
        for k, v in self.tasks.items():
            for d in v[0]:
                users.setdefault(d, []).append(k)
            if not waits[k]:
                open_.add(k)

        def came(d, at):
            for k in users.get(d, ()):
                waits[k] -= 1
                ready[k] = max(ready[k], at + (self.tasks[k][5] if d not in self.tasks else 0.0))
                if not waits[k]:
                    open_.add(k)

        index = {k: i for i, k in enumerate(self.tasks)}
        while open_:
            best = min(open_, key=lambda k: (max(ready[k], t), self.tasks[k][3], ready[k], index[k]))
            open_.remove(best)
            _, dur, sends, *_ = self.tasks[best]
            t = max(t, ready[best]) + dur
            came(best, t)
            for key, link, size, hops in sends:
                rate = 650e3 if link == "d2d" else 46.6e3
                begin = max(free.get(link, 0.0), t)
                wire = size * max(hops, 1) / rate
                free[link] = begin + wire
                came(key, begin + wire + (1.0 if link == "d2d" else 0.95 + 0.75 * hops))
            seq.append((best, t))
        assert len(seq) == len(self.tasks)
        return seq


def make_plan():
    plan = Plan()
    stream_tasks = {}
    plan.task("pack1", [], 1.5)
    plan.task("pack2", ["pack1"], 0.1, (), 2)
    plan.task("pack3", ["pack1"], 0.2, (), 2)
    for s, stream in enumerate(STREAMS):
        arr = arrivals_of(stream)
        leaves = leaves_of(arr)
        sends = {}
        for a, (parent, axis, step) in arr.items():
            key = ("w", s, *a)
            link = axis + ("+" if step > 0 else "-")
            cp = plan.copy(key, link, stream[1] * 256, abs(step), ("leaf", s) if a in leaves else key)
            sends.setdefault(parent, []).append(cp)
        pack = "pack1" if s in IN + BLEND else "pack2" if s in SE else "pack3"
        plan.task(("go", s), [pack], 0.03, sends[(0, 0)], 0, stream[5])
        for a in arr:
            if a not in leaves:
                plan.task(("recv", s, *a), [("w", s, *a), ("go", s)], 0.03, sends[a], 0, 0.0, stream[6])
        plan.task(("leaf", s), [("go", s), *[("w", s, *a) for a in leaves]], 0.03, (), 1)
        stream_tasks[s] = [("recv", s, *a) for a in arr if a not in leaves] + [("leaf", s)]

    def whole(which):
        return [t for s in which for t in stream_tasks[s]]

    plan.task("norm", ["pack1"], 0.45, (), 2)
    sq = [plan.copy(("sq", k), "d2d" if k == 4 else "q", 1024, 1) for k in range(1, NTP)]
    plan.task("in", ["norm", *whole(IN)], 0.9, sq, 2)
    plan.task("mask", ["pack1"], 0.03, (), 3)
    plan.task("mixed", ["in", "mask", *[("sq", k) for k in range(1, NTP)]], 0.45, (), 1)

    half = 65536

    def scatter(w, deps, dur):
        last = deps
        for k in (2, 1, 3, 0):
            cp = plan.copy(("p", w, k), "d2d", 2 * half, 1)
            plan.task(("part", w, k), last, dur, (cp,), 1)
            last = [("part", w, k)]
        cps = [plan.copy(("c", w, 2, h), "x-" if h else "x+", half, 1) for h in (0, 1)]
        plan.task(("sum2", w), [*last, ("p", w, 2)], dur + 0.1, cps, 1)
        last = [("sum2", w)]
        for k, h in ((1, 1), (3, 0), (1, 0), (3, 1)):
            cp = plan.copy(("c", w, k, h), "x-" if k == 3 else "x+", half, 1)
            need = [("c", w, 2, h)] if (k, h) in ((1, 0), (3, 1)) else []
            plan.task(("sum", w, k, h), [*last, *need, ("p", w, k)], dur * 0.6 + 0.1, (cp,), 1)
        plan.task(("own", w), [*last, ("p", w, 0)], dur, (), 2)
        return [("own", w)] + [("c", w, k, h) for k in (1, 3) for h in (0, 1)]

    after = scatter(0, ["mixed", *whole(BLEND)], 0.2)
    ag = [plan.copy(("ac", k, h), "x-" if k == 3 else "x+", half, 1) for k, h in ((1, 0), (3, 1), (1, 1), (3, 0))]
    ag.append(plan.copy(("ap", 0, 0), "d2d", 2 * half, 1))
    plan.task("stream", after, 0.2, ag, 1)
    got = [("ap", 0, 0)]
    for k, h in ((1, 0), (3, 1), (1, 1), (3, 0), (2, 0), (2, 1)):
        cps = []
        if (k, h) in ((1, 0), (3, 1)):
            cps.append(plan.copy(("ac", 2, h), "x-" if h else "x+", half, 1))
        cps.append(plan.copy(("ap", k, h), "d2d", half, 1))
        plan.task(("pass", k, h), [("ac", k, h), "stream"], 0.03, cps, 0)
        got += [("pass", k, h), ("ap", k, h)]
    plan.task("norm2", ["stream", *got], 0.5, (), 1)
    plan.task("hidden", ["norm2", *whole(SE)], 1.3, (), 1)
    after = scatter(1, ["hidden", *whole(CON)], 0.3)
    plan.task("out", after, 0.3, (), 1)
    return plan


def kernel(
    plan,
    seq,
    *refs,
):
    hbm, out_ref, rest = refs[: len(NAMES)], refs[len(NAMES)], refs[len(NAMES) + 1 :]
    local, rest = rest[: len(NAMES)], rest[len(NAMES) :]
    (
        g,
        normed,
        carrier,
        spread,
        sqbuf,
        opm,
        gated,
        active,
        psend,
        precv,
        csend,
        crecv,
        own,
        sbuf,
        scale,
        send_sem,
        recv_sem,
        load_sem,
    ) = rest
    (
        x_ref, gain1_ref, wprod_ref, sprod_ref, wplace_ref, splace_ref, gains_ref, op_ref, bias_ref,
        wblend_ref, sblend_ref, gain2_ref, wsw_ref, ssw_ref, wex_ref, sex_ref, wcon_ref, scon_ref,
    ) = local
    rep, fs, tp = lax.axis_index("rep"), lax.axis_index("fs"), lax.axis_index("tp")
    zl, y = fs // NY, lax.rem(fs, NY)
    x, core = tp // 2, lax.rem(tp, 2)
    z = rep * NZ + zl

    def at_z(d):
        zz = lax.rem(z + d + NREP * NZ, NREP * NZ)
        return {"rep": zz // NZ, "fs": lax.rem(zz, NZ) * NY + y}

    def at_y(d):
        return {"fs": zl * NY + lax.rem(y + d + NY, NY)}

    def at_tp(k):
        return {"tp": lax.rem(tp + k + NTP, NTP)}

    def at_x(k):
        return {"tp": lax.rem(x + k + NX, NX) * 2 + core}

    partner = {"tp": x * 2 + 1 - core}

    def slot(a):
        return lax.rem(zl - a[0] + NZ, NZ) * NY + lax.rem(y - a[1] + NY, NY)

    def send(key, src, dst, dev):
        pltpu.make_async_remote_copy(
            src_ref=src, dst_ref=dst, send_sem=send_sem.at[KINDS.index(key[0])], recv_sem=recv_sem.at[plan.copies[key]],
            device_id=dev, device_id_type=MESH,
        ).start()

    def arrive(key, dst, dev):
        pltpu.make_async_remote_copy(
            src_ref=dst, dst_ref=dst, send_sem=send_sem.at[KINDS.index(key[0])], recv_sem=recv_sem.at[plan.copies[key]],
            device_id=dev, device_id_type=MESH,
        ).wait_recv()

    arrs = [arrivals_of(s) for s in STREAMS]

    def block(s, a):
        return g.at[slot(a), pl.ds(STREAMS[s][0], STREAMS[s][1])]

    def forward(s, a):
        for b, (parent, axis, step) in arrs[s].items():
            if parent == a:
                send(("w", s, *b), block(s, a), block(s, a), at_z(step) if axis == "z" else at_y(step))

    zs = sorted({e * v[2] for a in arrs for v in a.values() if v[1] == "z" for e in (1, -1)})
    ys = sorted({(e * v[2]) % NY for a in arrs for v in a.values() if v[1] == "y" for e in (1, -1)})
    greet = [at_z(d) for d in zs] + [at_y(d) for d in ys] + [at_tp(k) for k in range(1, NTP)]
    barrier = pltpu.get_barrier_semaphore()
    for dev in greet:
        pl.semaphore_signal(barrier, inc=1, device_id=dev, device_id_type=MESH)

    def loading(name):
        i = NAMES.index(name)
        return pltpu.make_async_copy(hbm[i], local[i], load_sem.at[i])

    for name in LOADS:
        loading(name).start()

    def load(*names):
        for name in names:
            loading(name).wait()

    def pack1():
        load("wprod", "wplace", "wblend", "sblend")
        g[fs, R_PROD : R_PROD + 64, :] = wprod_ref[...].astype(BF16)
        g[fs, R_PLACE : R_PLACE + 64, :] = wplace_ref[...].astype(BF16)
        wb = wblend_ref[...].astype(BF16).astype(F32) * jnp.broadcast_to(sblend_ref[...], (128, 64)).T
        g[fs, R_BLEND : R_BLEND + 64, :] = wb.astype(BF16)
        pl.semaphore_wait(barrier, len(greet))

    def pack2():
        load("wsw", "wex", "ssw", "sex")
        for i, w in ((0, wsw_ref), (2, wex_ref)):
            for j in (0, 1):
                g[fs, R_SE + 64 * (i + j) : R_SE + 64 * (i + j + 1), :] = w[:, 128 * j : 128 * (j + 1)].astype(BF16)
        zero = jnp.zeros((64, 128), BF16)
        for i, w in ((4, wsw_ref), (5, wex_ref)):
            g[fs, R_SE + 64 * i : R_SE + 64 * (i + 1), :] = zero
            g[fs, R_SE + 64 * i : R_SE + 64 * (i + 1), 0:96] = w[:, 256:352].astype(BF16)
        scale[...] = jnp.zeros_like(scale)
        scale[0:1, 0:HID] = ssw_ref[...].reshape(1, HID)
        scale[1:2, 0:HID] = sex_ref[...].reshape(1, HID)

    def pack3():
        load("wcon", "scon")
        by = jnp.broadcast_to(scon_ref[...], (128, 64)).T[:, 0:1]
        wc = (wcon_ref[...].astype(BF16).astype(F32) * by).astype(BF16)
        g[fs, R_CON : R_CON + 64, :] = wc[:, 0:128]
        g[fs, R_CON + 64 : R_CON + 128, :] = wc[:, 128:256]
        g[fs, R_CON + 128 : R_CON + 192, :] = jnp.zeros((64, 128), BF16)
        g[fs, R_CON + 128 : R_CON + 192, 0:96] = wc[:, 256:352]

    def go(s):
        forward(s, (0, 0))

    def recv(s, dz, dy):
        _, axis, step = arrs[s][(dz, dy)]
        arrive(("w", s, dz, dy), block(s, (dz, dy)), at_z(-step) if axis == "z" else at_y(-step))
        forward(s, (dz, dy))

    def leaf(s):
        leaves = leaves_of(arrs[s])
        ref = g.at[0 : len(leaves), pl.ds(STREAMS[s][0], STREAMS[s][1])]
        arrive(("w", s, *leaves[0]), ref, at_y(1))

    def tile(row):
        return g[:, row : row + 64, :].reshape(DIM, 128)

    def norm():
        load("x", "gain1")
        v = x_ref[...].astype(F32)
        r = lax.rsqrt(jnp.mean(v * v, axis=-1, keepdims=True) + EPS)
        normed[...] = (v * r * gain1_ref[...]).astype(BF16)

    def enter():
        load("sprod", "splace")
        w = jnp.concatenate([tile(R_PROD), tile(R_PLACE)], axis=1)
        h = jnp.dot(normed[...], w, preferred_element_type=F32)
        sp = jax.nn.gelu(h[:, 128:256] * splace_ref[...])
        spread[...] = sp
        sqbuf[tp] = jnp.sum((sp * sp).T, axis=0, keepdims=True)
        for k in range(1, NTP):
            send(("sq", k), sqbuf.at[tp], sqbuf.at[tp], at_tp(k))
        carrier[...] = jax.nn.gelu(h[:, 0:128] * sprod_ref[...])

    def mask():
        load("op", "gains", "bias", "gain2")
        t = lax.broadcasted_iota(jnp.int32, (BLOCK, BLOCK), 0)
        s = lax.broadcasted_iota(jnp.int32, (BLOCK, BLOCK), 1)
        opm[...] = jnp.where(t >= s, op_ref[tp].astype(F32), 0.0).astype(BF16)

    def mixed():
        for k in range(1, NTP):
            src = lax.rem(tp - k + NTP, NTP)
            arrive(("sq", k), sqbuf.at[src], at_tp(-k))
        total = jnp.sum(sqbuf[...], axis=0)
        r = lax.rsqrt(total / CH + EPS)
        r = jnp.broadcast_to(r, (128, TOK)).T
        sn = (spread[...] * r * gains_ref[...]).astype(BF16)
        bias = jnp.broadcast_to(bias_ref[pl.ds(tp, 1), :], (BLOCK, BLOCK)).T
        w = opm[...]
        for n in range(TOK // BLOCK):
            rows = slice(n * BLOCK, (n + 1) * BLOCK)
            m = jnp.dot(w, sn[rows], preferred_element_type=F32) + bias
            gated[rows, :] = (carrier[rows, :] * m).astype(BF16)

    nt = (((1,), (1,)), ((), ()))

    def product(w, d, r=slice(None)):
        if w == 0:
            b = g[pl.ds(4 * d, 4), R_BLEND : R_BLEND + 64, :].reshape(256, 128)
            return lax.dot_general(gated[r, :], b, nt, preferred_element_type=F32)
        cols = [g[pl.ds(4 * d, 4), R_CON + 64 * j : R_CON + 64 * (j + 1), :].reshape(256, 128) for j in range(3)]
        return lax.dot_general(active[r, :], jnp.concatenate(cols, axis=1), nt, preferred_element_type=F32)

    def chip(k):
        return lax.rem(x + k, NX) * 2

    def part(w, k):
        psend[w, k] = product(w, chip(k) + 1 - core).astype(BF16)
        send(("p", w, k), psend.at[w, k], precv.at[w, k], partner)

    def rows(h):
        return slice(128 * h, 128 * (h + 1))

    def sum2(w):
        v = product(w, chip(2) + core)
        arrive(("p", w, 2), precv.at[w, 2], partner)
        csend[w, 0] = (v + precv[w, 2].astype(F32)).astype(BF16)
        for h in (0, 1):
            send(("c", w, 2, h), csend.at[w, 0, rows(h)], crecv.at[w, 0, rows(h)], at_x(-1 if h else 1))

    def add(w, k, h):
        v = product(w, chip(k) + core, rows(h))
        if (k, h) in ((1, 1), (3, 0)):
            arrive(("p", w, k), precv.at[w, k], partner)
        v = v + precv[w, k, rows(h)].astype(F32)
        if (k, h) in ((1, 0), (3, 1)):
            arrive(("c", w, 2, h), crecv.at[w, 0, rows(h)], at_x(1 if h else -1))
            v = v + crecv[w, 0, rows(h)].astype(F32)
        i = 1 if k == 1 else 2
        csend[w, i, rows(h)] = v.astype(BF16)
        send(("c", w, k, h), csend.at[w, i, rows(h)], crecv.at[w, i, rows(h)], at_x(k))

    def keep(w):
        v = product(w, chip(0) + core)
        arrive(("p", w, 0), precv.at[w, 0], partner)
        own[...] = v + precv[w, 0].astype(F32)

    def total(w):
        v = own[...]
        for k in (1, 3):
            i = 1 if k == 1 else 2
            for h in (0, 1):
                arrive(("c", w, k, h), crecv.at[w, i, rows(h)], at_x(-k))
            v = v + crecv[w, i].astype(F32)
        return v

    def stream():
        mine = x_ref[:, pl.ds(pl.multiple_of(tp * 256, 256), 256)].astype(F32)
        sbuf[tp] = (mine + total(0)).astype(BF16)
        for k, h in ((1, 0), (3, 1), (1, 1), (3, 0)):
            send(("ac", k, h), sbuf.at[tp, rows(h)], sbuf.at[tp, rows(h)], at_x(k))
        send(("ap", 0, 0), sbuf.at[tp], sbuf.at[tp], partner)

    def relay(k, h):
        d = lax.rem(x - k + NX, NX) * 2 + core
        ref = sbuf.at[d, rows(h)]
        arrive(("ac", k, h), ref, at_x(-k) if k != 2 else at_x(1 if h else -1))
        if (k, h) in ((1, 0), (3, 1)):
            send(("ac", 2, h), ref, ref, at_x(-1 if h else 1))
        send(("ap", k, h), ref, ref, partner)

    def norm2():
        for k in range(4):
            d = lax.rem(x - k + NX, NX) * 2 + 1 - core
            if k == 0:
                arrive(("ap", 0, 0), sbuf.at[d], partner)
            else:
                for h in (0, 1):
                    arrive(("ap", k, h), sbuf.at[d, rows(h)], partner)
        sq = jnp.zeros((TOK, 256), F32)
        for d in range(NTP):
            v = sbuf[d].astype(F32)
            sq = sq + v * v
        r = lax.rsqrt(jnp.sum(sq, axis=-1, keepdims=True) / DIM + EPS)
        for d in range(NTP):
            cols = slice(256 * d, 256 * (d + 1))
            normed[:, cols] = (sbuf[d].astype(F32) * r * gain2_ref[:, cols]).astype(BF16)

    def hidden():
        for j, (a, b) in enumerate(((0, 2), (1, 3), (4, 5))):
            w = jnp.concatenate([tile(R_SE + 64 * a), tile(R_SE + 64 * b)], axis=1)
            h = jnp.dot(normed[...], w, preferred_element_type=F32)
            cols = slice(128 * j, 128 * (j + 1))
            gate = h[:, 0:128] * scale[0:1, cols]
            up = h[:, 128:256] * scale[1:2, cols]
            active[:, cols] = (gate / (1.0 + jnp.exp(-gate)) * up).astype(BF16)

    def out():
        out_ref[...] = (sbuf[tp].astype(F32) + total(1)).astype(BF16)

    run = {
        "pack1": pack1, "pack2": pack2, "pack3": pack3, "go": go, "norm": norm, "in": enter, "mask": mask, "mixed": mixed, "stream": stream,
        "norm2": norm2, "hidden": hidden, "out": out, "recv": recv, "leaf": leaf, "part": part, "sum": add, "sum2": sum2, "own": keep, "pass": relay,
    }
    for key, _ in seq:
        if isinstance(key, tuple):
            run[key[0]](*key[1:])
        else:
            run[key]()
    for i, all_sent in enumerate((g.at[0:31], sqbuf.at[0:7], psend, csend, sbuf.at[0:3], sbuf.at[0:4])):
        pltpu.make_async_copy(all_sent, all_sent, send_sem.at[i]).wait()


def on_device(*args):
    plan = make_plan()
    seq = plan.order()
    n = len(plan.groups)
    args = list(args)
    for i in (NAMES.index("wblend"), NAMES.index("wcon")):
        args[i] = args[i].T
    args = [a.reshape(1, -1) if a.ndim == 1 and a.size != HID else a for a in args]
    return pl.pallas_call(
        functools.partial(kernel, plan, seq),
        out_shape=jax.ShapeDtypeStruct((TOK, 256), BF16),
        in_specs=[pl.BlockSpec(memory_space=pltpu.HBM)] * len(args),
        out_specs=pl.BlockSpec(memory_space=pltpu.VMEM),
        scratch_shapes=[
            *[pltpu.VMEM(a.shape, a.dtype) for a in args],
            pltpu.VMEM((NY * NZ, R_ALL, 128), BF16),
            pltpu.VMEM((TOK, DIM), BF16),
            pltpu.VMEM((TOK, 128), F32),
            pltpu.VMEM((TOK, 128), F32),
            pltpu.VMEM((NTP, 1, TOK), F32),
            pltpu.VMEM((BLOCK, BLOCK), BF16),
            pltpu.VMEM((TOK, 128), BF16),
            pltpu.VMEM((TOK, 384), BF16),
            pltpu.VMEM((2, 4, TOK, 256), BF16),
            pltpu.VMEM((2, 4, TOK, 256), BF16),
            pltpu.VMEM((2, 3, TOK, 256), BF16),
            pltpu.VMEM((2, 3, TOK, 256), BF16),
            pltpu.VMEM((TOK, 256), F32),
            pltpu.VMEM((NTP, TOK, 256), BF16),
            pltpu.VMEM((8, 384), F32),
            pltpu.SemaphoreType.DMA((len(KINDS),)),
            pltpu.SemaphoreType.DMA((n,)),
            pltpu.SemaphoreType.DMA((len(args),)),
        ],
        compiler_params=pltpu.CompilerParams(
            collective_id=0, has_side_effects=True, vmem_limit_bytes=67043328
        ),
        name="layer",
    )(*args)


def solution(mesh):
    return jax.shard_map(
        on_device,
        mesh=mesh,
        in_specs=(
            P(("rep", "fs"), None),
            P(),
            P("fs", "tp"),
            P("tp"),
            P("fs", "tp"),
            P("tp"),
            P("tp"),
            P(),
            P(),
            P("tp", "fs"),
            P("fs"),
            P(),
            P("fs", "tp"),
            P("tp"),
            P("fs", "tp"),
            P("tp"),
            P("tp", "fs"),
            P("fs"),
        ),
        out_specs=P(("rep", "fs"), "tp"),
        check_vma=False,
    )
```

time: 102 us -> 79.7 us (0.78)
  Pallas kernels: 90.3 us -> 77.8 us
  local copies, waits for them, and re-layouts: 11.5 us -> 1.57 us
    pallas_call x1, Pallas kernels: 90.3 us -> 77.8 us  [on_device(): pl.pallas_call(functools.partial(kernel, plan, seq), out_shape=jax.ShapeD...]
    unnamed x31 -> x1, local copies, waits for them, and re-layouts: 10.1 us -> 1.57 us
    reshape x2 -> x0, local copies, waits for them, and re-layouts: 1.41 us -> none  [on_device(): args = [a.reshape(1, -1) if a.ndim == 1 else a for a in args]]
where the time goes in v2:
time: 79.7 us; the launch traced here: 79.4 us
  Pallas kernels  77.8 us (98%)
  local copies, waits for them, and re-layouts  1.57 us (2%)
    pallas_call x1, Pallas kernels, on_device(): pl.pallas_call(functools.partial(kernel, plan, seq), out_shape=jax.ShapeD...  77.8 us

profile of v2, /device:TPU:1, one launch (start us, length us, event | category | flops | bytes accessed | tf_op | source)
XLA Modules:
  0.0 79.4 jit_solution(533102108844133114)
XLA Ops:
  0.0 77.8 %layer.1 = bf16[256,256]{1,0:T(8,128)(2,1)} custom-call(bf16[256,2048]{1,0:T(8,128)(2,1)} %refs_0_.1, f32[1,2048]{1,0:T(1,128)} %bitcast.11, f32[64,128]{1,0:T(8,128)} %refs_2_.1, f32[1,128]{1,0:T(1,128)} %bitcast.13, f32[64,128]{1,0:T(8,128)} %refs_4_.1, f32[1,128]{1,0:T(1,128)} %bitcast.14, f32[1,128]{1,0:T(1,128)} %bitcast.15, ...), custom_call_target="tpu_custom_call" | custom-call | tf_op jit(solution)/shard_map/layer/pallas_call | solution.py:496
  77.8 1.6 %copy.20 = bf16[256,256]{1,0:T(8,128)(2,1)} copy(bf16[256,256]{1,0:T(8,128)(2,1)} %layer.1) | data formatting | bytes 262144

commit v3 on v2

--- a/solution.py
+++ b/solution.py
@@ -19,7 +19,8 @@
 HID = 352
 NY, NZ, NX, NTP, NREP = 4, 8, 4, 8, 4
 
-R_PROD, R_PLACE, R_BLEND, R_SE, R_CON, R_ALL = 0, 64, 128, 192, 576, 768
+R_PROD, R_PLACE, R_BLEND, R_SE, R_CON, R_ALL = 0, 64, 128, 192, 576, 720
+R_TAIL = R_SE + 256
 
 RING4 = {1: 0, 2: 1, 3: 2, 4: 3, -1: 0, -2: -1, -3: -2}
 RING3 = {1: 0, 2: 1, 3: 2, -1: 0, -2: -1, -3: -2, -4: -3}
@@ -43,15 +44,14 @@
 )
 
 STREAMS = (
-    (0, 64, "z", JUMP4, YDN, 0.0, 0.0),
-    (64, 64, "z", JUMP3, YUP, 0.0, 0.0),
-    (128, 64, "z", JUMP3, YDN, 2.5, 0.0),
-    (192, 128, "z", RING4, YUP, 12.2, 1.0),
-    (320, 128, "z", JUMP3, YDN, 13.6, 1.0),
-    (448, 128, "y", RING3, YUP, 0, 1.0),
-    (576, 192, "y", RING4, YUP, 13.2, 1.0),
+    (0, 64, "z", JUMP3, YDN, 0.0, 1.0),
+    (64, 64, "y", JUMP4, YUP, 0.0, 0.5),
+    (128, 64, "z", JUMP3, YDN, 0.0, 0.5),
+    (192, 192, "z", RING4, YUP, 8.6, 1.0),
+    (384, 192, "y", RING4, YUP, 12.7, 1.0),
+    (576, 144, "z", JUMP3, YDN, 14.4, 2.0),
 )
-IN, BLEND, SE, CON = (0, 1), (2,), (3, 4, 5), (6,)
+IN, BLEND, SE, CON = (0, 1), (2,), (3, 4), (5,)
 
 
 def order_of(tree):
@@ -81,6 +81,9 @@
     return [a for a in arrivals if a not in parents]
 
 
+LATENCY = {"d2d": 0.6, "q": 2.9, "z+": 1.05, "z-": 1.05, "y+": 1.05, "y-": 1.05, "x+": 1.25, "x-": 1.25}
+
+
 class Plan:
     def __init__(self):
         self.tasks = {}
@@ -119,11 +122,11 @@
             t = max(t, ready[best]) + dur
             came(best, t)
             for key, link, size, hops in sends:
-                rate = 650e3 if link == "d2d" else 46.6e3
+                rate = 650e3 if link == "d2d" else 45e3
                 begin = max(free.get(link, 0.0), t)
                 wire = size * max(hops, 1) / rate
                 free[link] = begin + wire
-                came(key, begin + wire + (1.0 if link == "d2d" else 0.95 + 0.75 * hops))
+                came(key, begin + wire + LATENCY.get(link, 0.5) + 0.75 * hops)
             seq.append((best, t))
         assert len(seq) == len(self.tasks)
         return seq
@@ -133,8 +136,7 @@
     plan = Plan()
     stream_tasks = {}
     plan.task("pack1", [], 1.5)
-    plan.task("pack2", ["pack1"], 0.1, (), 2)
-    plan.task("pack3", ["pack1"], 0.2, (), 2)
+    plan.task("pack2", ["pack1"], 0.3, (), 2)
     for s, stream in enumerate(STREAMS):
         arr = arrivals_of(stream)
         leaves = leaves_of(arr)
@@ -144,7 +146,7 @@
             link = axis + ("+" if step > 0 else "-")
             cp = plan.copy(key, link, stream[1] * 256, abs(step), ("leaf", s) if a in leaves else key)
             sends.setdefault(parent, []).append(cp)
-        pack = "pack1" if s in IN + BLEND else "pack2" if s in SE else "pack3"
+        pack = "pack1" if s in IN + BLEND else "pack2"
         plan.task(("go", s), [pack], 0.03, sends[(0, 0)], 0, stream[5])
         for a in arr:
             if a not in leaves:
@@ -157,9 +159,10 @@
 
     plan.task("norm", ["pack1"], 0.45, (), 2)
     sq = [plan.copy(("sq", k), "d2d" if k == 4 else "q", 1024, 1) for k in range(1, NTP)]
-    plan.task("in", ["norm", *whole(IN)], 0.9, sq, 2)
+    plan.task("spread", ["norm", *whole(IN[1:])], 0.6, sq, 1)
+    plan.task("carrier", ["norm", *whole(IN[:1])], 0.5, (), 2)
     plan.task("mask", ["pack1"], 0.03, (), 3)
-    plan.task("mixed", ["in", "mask", *[("sq", k) for k in range(1, NTP)]], 0.45, (), 1)
+    plan.task("mixed", ["spread", "carrier", "mask", *[("sq", k) for k in range(1, NTP)]], 0.45, (), 1)
 
     half = 65536
 
@@ -170,13 +173,12 @@
             plan.task(("part", w, k), last, dur, (cp,), 1)
             last = [("part", w, k)]
         cps = [plan.copy(("c", w, 2, h), "x-" if h else "x+", half, 1) for h in (0, 1)]
-        plan.task(("sum2", w), [*last, ("p", w, 2)], dur + 0.1, cps, 1)
-        last = [("sum2", w)]
+        plan.task(("sum2", w), [("part", w, 2), ("p", w, 2)], dur + 0.1, cps, 1)
         for k, h in ((1, 1), (3, 0), (1, 0), (3, 1)):
             cp = plan.copy(("c", w, k, h), "x-" if k == 3 else "x+", half, 1)
-            need = [("c", w, 2, h)] if (k, h) in ((1, 0), (3, 1)) else []
-            plan.task(("sum", w, k, h), [*last, *need, ("p", w, k)], dur * 0.6 + 0.1, (cp,), 1)
-        plan.task(("own", w), [*last, ("p", w, 0)], dur, (), 2)
+            need = [("c", w, 2, h), ("sum", w, k, 1 - h)] if (k, h) in ((1, 0), (3, 1)) else [("sum2", w)]
+            plan.task(("sum", w, k, h), [("part", w, k), *need, ("p", w, k)], dur * 0.6 + 0.1, (cp,), 1)
+        plan.task(("own", w), [("part", w, 0), ("p", w, 0)], dur, (), 2)
         return [("own", w)] + [("c", w, k, h) for k in (1, 3) for h in (0, 1)]
 
     after = scatter(0, ["mixed", *whole(BLEND)], 0.2)
@@ -193,7 +195,8 @@
         got += [("pass", k, h), ("ap", k, h)]
     plan.task("norm2", ["stream", *got], 0.5, (), 1)
     plan.task("hidden", ["norm2", *whole(SE)], 1.3, (), 1)
-    after = scatter(1, ["hidden", *whole(CON)], 0.3)
+    plan.task("unpack", [*whole(SE[-1:]), *whole(CON)], 0.5, (), 1)
+    after = scatter(1, ["hidden", "unpack"], 0.3)
     plan.task("out", after, 0.3, (), 1)
     return plan
 
@@ -210,6 +213,7 @@
         normed,
         carrier,
         spread,
+        tail,
         sqbuf,
         opm,
         gated,
@@ -305,22 +309,26 @@
         for i, w in ((0, wsw_ref), (2, wex_ref)):
             for j in (0, 1):
                 g[fs, R_SE + 64 * (i + j) : R_SE + 64 * (i + j + 1), :] = w[:, 128 * j : 128 * (j + 1)].astype(BF16)
-        zero = jnp.zeros((64, 128), BF16)
-        for i, w in ((4, wsw_ref), (5, wex_ref)):
-            g[fs, R_SE + 64 * i : R_SE + 64 * (i + 1), :] = zero
-            g[fs, R_SE + 64 * i : R_SE + 64 * (i + 1), 0:96] = w[:, 256:352].astype(BF16)
+        load("wcon", "scon")
+        by = jnp.broadcast_to(scon_ref[...], (128, 64)).T[:, 0:1]
+        wc = (wcon_ref[...].astype(BF16).astype(F32) * by).astype(BF16)
+        for i, w in ((0, wsw_ref), (1, wex_ref)):
+            at = pl.ds(R_TAIL + 64 * i, 64)
+            g[fs, at, 0:96] = w[:, 256:352].astype(BF16)
+            g[fs, at, 96:128] = wc[:, 256 + 32 * i : 288 + 32 * i]
+        g[fs, R_CON : R_CON + 64, :] = wc[:, 0:128]
+        g[fs, R_CON + 64 : R_CON + 128, :] = wc[:, 128:256]
+        for q in range(4):
+            g[fs, R_CON + 128 : R_CON + 144, 32 * q : 32 * (q + 1)] = wc[16 * q : 16 * (q + 1), 320:352]
         scale[...] = jnp.zeros_like(scale)
         scale[0:1, 0:HID] = ssw_ref[...].reshape(1, HID)
         scale[1:2, 0:HID] = sex_ref[...].reshape(1, HID)
 
-    def pack3():
-        load("wcon", "scon")
-        by = jnp.broadcast_to(scon_ref[...], (128, 64)).T[:, 0:1]
-        wc = (wcon_ref[...].astype(BF16).astype(F32) * by).astype(BF16)
-        g[fs, R_CON : R_CON + 64, :] = wc[:, 0:128]
-        g[fs, R_CON + 64 : R_CON + 128, :] = wc[:, 128:256]
-        g[fs, R_CON + 128 : R_CON + 192, :] = jnp.zeros((64, 128), BF16)
-        g[fs, R_CON + 128 : R_CON + 192, 0:96] = wc[:, 256:352]
+    def unpack():
+        for i in (0, 1):
+            tail[:, :, 32 * i : 32 * (i + 1)] = g[:, R_TAIL + 64 * i : R_TAIL + 64 * (i + 1), 96:128]
+        for q in range(4):
+            tail[:, 16 * q : 16 * (q + 1), 64:96] = g[:, R_CON + 128 : R_CON + 144, 32 * q : 32 * (q + 1)]
 
     def go(s):
         forward(s, (0, 0))
@@ -344,19 +352,23 @@
         r = lax.rsqrt(jnp.mean(v * v, axis=-1, keepdims=True) + EPS)
         normed[...] = (v * r * gain1_ref[...]).astype(BF16)
 
-    def enter():
-        load("sprod", "splace")
-        w = jnp.concatenate([tile(R_PROD), tile(R_PLACE)], axis=1)
-        h = jnp.dot(normed[...], w, preferred_element_type=F32)
-        sp = jax.nn.gelu(h[:, 128:256] * splace_ref[...])
+    def spreading():
+        load("splace")
+        h = jnp.dot(normed[...], tile(R_PLACE), preferred_element_type=F32)
+        sp = jax.nn.gelu(h * splace_ref[...])
         spread[...] = sp
         sqbuf[tp] = jnp.sum((sp * sp).T, axis=0, keepdims=True)
         for k in range(1, NTP):
             send(("sq", k), sqbuf.at[tp], sqbuf.at[tp], at_tp(k))
-        carrier[...] = jax.nn.gelu(h[:, 0:128] * sprod_ref[...])
+
+    def carry():
+        load("sprod")
+        h = jnp.dot(normed[...], tile(R_PROD), preferred_element_type=F32)
+        carrier[...] = jax.nn.gelu(h * sprod_ref[...])
 
     def mask():
         load("op", "gains", "bias", "gain2")
+        tail[...] = jnp.zeros_like(tail)
         t = lax.broadcasted_iota(jnp.int32, (BLOCK, BLOCK), 0)
         s = lax.broadcasted_iota(jnp.int32, (BLOCK, BLOCK), 1)
         opm[...] = jnp.where(t >= s, op_ref[tp].astype(F32), 0.0).astype(BF16)
@@ -382,7 +394,8 @@
         if w == 0:
             b = g[pl.ds(4 * d, 4), R_BLEND : R_BLEND + 64, :].reshape(256, 128)
             return lax.dot_general(gated[r, :], b, nt, preferred_element_type=F32)
-        cols = [g[pl.ds(4 * d, 4), R_CON + 64 * j : R_CON + 64 * (j + 1), :].reshape(256, 128) for j in range(3)]
+        cols = [g[pl.ds(4 * d, 4), R_CON + 64 * j : R_CON + 64 * (j + 1), :].reshape(256, 128) for j in (0, 1)]
+        cols.append(tail[pl.ds(4 * d, 4)].reshape(256, 128))
         return lax.dot_general(active[r, :], jnp.concatenate(cols, axis=1), nt, preferred_element_type=F32)
 
     def chip(k):
@@ -473,7 +486,7 @@
         out_ref[...] = (sbuf[tp].astype(F32) + total(1)).astype(BF16)
 
     run = {
-        "pack1": pack1, "pack2": pack2, "pack3": pack3, "go": go, "norm": norm, "in": enter, "mask": mask, "mixed": mixed, "stream": stream,
+        "pack1": pack1, "pack2": pack2, "go": go, "norm": norm, "spread": spreading, "carrier": carry, "unpack": unpack, "mask": mask, "mixed": mixed, "stream": stream,
         "norm2": norm2, "hidden": hidden, "out": out, "recv": recv, "leaf": leaf, "part": part, "sum": add, "sum2": sum2, "own": keep, "pass": relay,
     }
     for key, _ in seq:
@@ -504,6 +517,7 @@
             pltpu.VMEM((TOK, DIM), BF16),
             pltpu.VMEM((TOK, 128), F32),
             pltpu.VMEM((TOK, 128), F32),
+            pltpu.VMEM((NY * NZ, 64, 128), BF16),
             pltpu.VMEM((NTP, 1, TOK), F32),
             pltpu.VMEM((BLOCK, BLOCK), BF16),
             pltpu.VMEM((TOK, 128), BF16),

time: 79.7 us -> 76.5 us (0.960)
  Pallas kernels: 77.8 us -> 74.8 us
    pallas_call x1, Pallas kernels: 77.8 us -> 74.8 us  [on_device(): pl.pallas_call(functools.partial(kernel, plan, seq), out_shape=jax.ShapeD...]
where the time goes in v3:
time: 76.5 us; the launch traced here: 76.3 us
  Pallas kernels  74.8 us (98%)
  local copies, waits for them, and re-layouts  1.57 us (2%)
    pallas_call x1, Pallas kernels, on_device(): pl.pallas_call(functools.partial(kernel, plan, seq), out_shape=jax.ShapeD...  74.8 us
    unnamed x1, local copies, waits for them, and re-layouts  1.57 us

profile of v3, /device:TPU:1, one launch (start us, length us, event | category | flops | bytes accessed | tf_op | source)
XLA Modules:
  0.0 76.3 jit_solution(12331025374126023792)
XLA Ops:
  0.0 74.8 %layer.1 = bf16[256,256]{1,0:T(8,128)(2,1)} custom-call(bf16[256,2048]{1,0:T(8,128)(2,1)} %refs_0_.1, f32[1,2048]{1,0:T(1,128)} %bitcast.11, f32[64,128]{1,0:T(8,128)} %refs_2_.1, f32[1,128]{1,0:T(1,128)} %bitcast.13, f32[64,128]{1,0:T(8,128)} %refs_4_.1, f32[1,128]{1,0:T(1,128)} %bitcast.14, f32[1,128]{1,0:T(1,128)} %bitcast.15, ...), custom_call_target="tpu_custom_call" | custom-call | tf_op jit(solution)/shard_map/layer/pallas_call | solution.py:509
  74.8 1.6 %copy.20 = bf16[256,256]{1,0:T(8,128)(2,1)} copy(bf16[256,256]{1,0:T(8,128)(2,1)} %layer.1) | data formatting | bytes 262144

commit v4 on v3

--- a/solution.py
+++ b/solution.py
@@ -47,9 +47,9 @@
     (0, 64, "z", JUMP3, YDN, 0.0, 1.0),
     (64, 64, "y", JUMP4, YUP, 0.0, 0.5),
     (128, 64, "z", JUMP3, YDN, 0.0, 0.5),
-    (192, 192, "z", RING4, YUP, 8.6, 1.0),
-    (384, 192, "y", RING4, YUP, 12.7, 1.0),
-    (576, 144, "z", JUMP3, YDN, 14.4, 2.0),
+    (192, 192, "z", RING4, YUP, 10.6, 1.0),
+    (384, 192, "y", RING4, YUP, 14.7, 1.0),
+    (576, 144, "z", JUMP3, YDN, 16.4, 2.0),
 )
 IN, BLEND, SE, CON = (0, 1), (2,), (3, 4), (5,)
 
@@ -136,7 +136,8 @@
     plan = Plan()
     stream_tasks = {}
     plan.task("pack1", [], 1.5)
-    plan.task("pack2", ["pack1"], 0.3, (), 2)
+    plan.task("packb", ["pack1"], 0.1, (), 0)
+    plan.task("pack2", ["packb"], 0.3, (), 2)
     for s, stream in enumerate(STREAMS):
         arr = arrivals_of(stream)
         leaves = leaves_of(arr)
@@ -146,7 +147,7 @@
             link = axis + ("+" if step > 0 else "-")
             cp = plan.copy(key, link, stream[1] * 256, abs(step), ("leaf", s) if a in leaves else key)
             sends.setdefault(parent, []).append(cp)
-        pack = "pack1" if s in IN + BLEND else "pack2"
+        pack = "pack1" if s in IN else "packb" if s in BLEND else "pack2"
         plan.task(("go", s), [pack], 0.03, sends[(0, 0)], 0, stream[5])
         for a in arr:
             if a not in leaves:
@@ -297,12 +298,15 @@
             loading(name).wait()
 
     def pack1():
-        load("wprod", "wplace", "wblend", "sblend")
+        load("wprod", "wplace")
         g[fs, R_PROD : R_PROD + 64, :] = wprod_ref[...].astype(BF16)
         g[fs, R_PLACE : R_PLACE + 64, :] = wplace_ref[...].astype(BF16)
+        pl.semaphore_wait(barrier, len(greet))
+
+    def packb():
+        load("wblend", "sblend")
         wb = wblend_ref[...].astype(BF16).astype(F32) * jnp.broadcast_to(sblend_ref[...], (128, 64)).T
         g[fs, R_BLEND : R_BLEND + 64, :] = wb.astype(BF16)
-        pl.semaphore_wait(barrier, len(greet))
 
     def pack2():
         load("wsw", "wex", "ssw", "sex")
@@ -486,7 +490,7 @@
         out_ref[...] = (sbuf[tp].astype(F32) + total(1)).astype(BF16)
 
     run = {
-        "pack1": pack1, "pack2": pack2, "go": go, "norm": norm, "spread": spreading, "carrier": carry, "unpack": unpack, "mask": mask, "mixed": mixed, "stream": stream,
+        "pack1": pack1, "packb": packb, "pack2": pack2, "go": go, "norm": norm, "spread": spreading, "carrier": carry, "unpack": unpack, "mask": mask, "mixed": mixed, "stream": stream,
         "norm2": norm2, "hidden": hidden, "out": out, "recv": recv, "leaf": leaf, "part": part, "sum": add, "sum2": sum2, "own": keep, "pass": relay,
     }
     for key, _ in seq:

time: 76.5 us -> 76.7 us (level)
  no operation moved by 1% of the time
where the time goes in v4:
time: 76.7 us; the launch traced here: 76.4 us
  Pallas kernels  74.8 us (98%)
  local copies, waits for them, and re-layouts  1.57 us (2%)
    pallas_call x1, Pallas kernels, on_device(): pl.pallas_call(functools.partial(kernel, plan, seq), out_shape=jax.ShapeD...  74.8 us
    unnamed x1, local copies, waits for them, and re-layouts  1.57 us

profile of v4, /device:TPU:1, one launch (start us, length us, event | category | flops | bytes accessed | tf_op | source)
XLA Modules:
  0.0 76.4 jit_solution(1747215222796487940)
XLA Ops:
  0.0 74.8 %layer.1 = bf16[256,256]{1,0:T(8,128)(2,1)} custom-call(bf16[256,2048]{1,0:T(8,128)(2,1)} %refs_0_.1, f32[1,2048]{1,0:T(1,128)} %bitcast.11, f32[64,128]{1,0:T(8,128)} %refs_2_.1, f32[1,128]{1,0:T(1,128)} %bitcast.13, f32[64,128]{1,0:T(8,128)} %refs_4_.1, f32[1,128]{1,0:T(1,128)} %bitcast.14, f32[1,128]{1,0:T(1,128)} %bitcast.15, ...), custom_call_target="tpu_custom_call" | custom-call | tf_op jit(solution)/shard_map/layer/pallas_call | solution.py:513
  74.8 1.6 %copy.20 = bf16[256,256]{1,0:T(8,128)(2,1)} copy(bf16[256,256]{1,0:T(8,128)(2,1)} %layer.1) | data formatting | bytes 262144
